TPU v7x, 32 devices: a whole 2x2x4 slice. The times are simulated.
32 devices in a mesh: fs: 8 (over z, y), tp: 4 (over x, core).
Axes of the slice: x: 2, y: 2, z: 4, core: 2. Of those that a mesh axis runs over, the one named last changes fastest.
Arguments:
- prompt: bfloat16 [4096, 2048], P(('fs', 'tp')), may hold values from -6 to 6
- norm_gain: float32 [2048], P('fs'), may hold values from 0.1 to 1.9
- up_trained: float32 [2048, 8192], P('fs', 'tp'), may hold values from -0.125 to 0.125
- down_trained: float32 [2048, 8192], P('fs', 'tp'), may hold values from -0.0625 to 0.0625
Outputs:
- up_served: bfloat16 [2048, 8192], P(None, 'tp')
- down_served: bfloat16 [8192, 2048], P('tp')
- mixed: bfloat16 [4096, 2048], P(('fs', 'tp'))
All inputs are finite; a program needn't handle non-finite values.
Results may differ from a plain program's by a relative error of at most 0.014.
Values may be sent and summed in bfloat16 or wider, within the bound.
A program may use at most 128 MiB of HBM per device.

v0:
```python
import jax
import jax.numpy as jnp
from jax import lax
from jax.sharding import PartitionSpec as P


def shards(prompt, norm_gain, up_trained, down_trained):
    up_local = (norm_gain[:, None] * up_trained).astype(jnp.bfloat16)
    down_local = down_trained.astype(jnp.bfloat16)
    values = prompt.astype(jnp.float32)
    scale = lax.rsqrt(jnp.mean(values * values, axis=-1, keepdims=True) + 1e-06)
    normed = (values * scale).astype(jnp.bfloat16)
    group_rows = lax.all_gather(normed, "tp", axis=0, tiled=True)
    pieces = (
        lax.all_gather(up_local, "fs", axis=0, tiled=True),
        lax.all_gather(down_local, "fs", axis=0, tiled=True),
    )
    pre = jnp.dot(group_rows, pieces[0], preferred_element_type=jnp.float32)
    up_buffer = pieces[0]
    down_buffer = pieces[1]
    pre, up_whole, down_whole = (pre, up_buffer, down_buffer)
    hidden = jnp.square(jax.nn.relu(pre)).astype(jnp.bfloat16)
    down_served = jnp.transpose(down_whole)
    mixed = lax.psum_scatter(
        jnp.dot(hidden, down_served, preferred_element_type=jnp.float32).astype(jnp.bfloat16),
        "tp",
        scatter_dimension=0,
        tiled=True,
    )
    return (up_whole, down_served, mixed)


def solution(mesh):
    return jax.shard_map(
        shards,
        mesh=mesh,
        in_specs=(P(("fs", "tp"), None), P("fs"), P("fs", "tp"), P("fs", "tp")),
        out_specs=(P(None, "tp"), P("tp", None), P(("fs", "tp"), None)),
        check_vma=False,
    )
```

profile of v0, /device:TPU:0, one launch (start us, length us, event | category | flops | bytes accessed | tf_op | source)
XLA Modules:
  0.0 358.5 jit_solution(13753829205279300968)
XLA Ops:
  7.2 0.0 copy-start
  7.2 0.0 all-gather.8.cloned.1.call-start
  7.2 1.4 fusion
  8.6 2.0 fusion.1
  10.6 0.0 all-gather.8.cloned.1.call-update
  10.6 0.0 all-gather.4.cloned.1.call-start
  10.7 2.7 multiply_convert_fusion.1
  13.4 0.0 all-gather.4.cloned.1.call-update
  13.4 0.0 all-gather.6.cloned.1.call-start
  13.5 0.0 copy-done
  13.5 1.4 copy.7
  14.9 0.0 all-gather.6.cloned.1.call-update
  14.9 0.0 reduce-scatter.2.cloned.1.call-start
  14.9 21.1 %all-gather.8.cloned.1.call-done = bf16[512,2048]{1,0:T(8,128)(2,1)} async-done(((bf16[128,2048]{1,0:T(8,128)(2,1)}), bf16[512,2048]{1,0:T(8,128)(2,1)}) %all-gather.8.cloned.1.call-update) | async-done | bytes 2097168 | tf_op jit(solution)/shard_map/all_gather | solution.py:13
  36.1 127.2 %all-gather.4.cloned.1.call-done = bf16[2048,2048]{1,0:T(8,128)(2,1)} async-done(((bf16[256,2048]{1,0:T(8,128)(2,1)}), bf16[2048,2048]{1,0:T(8,128)(2,1)}) %all-gather.4.cloned.1.call-update) | async-done | bytes 8388624 | tf_op jit(solution)/shard_map/all_gather | solution.py:15
  163.3 125.8 %all-gather.6.cloned.1.call-done = bf16[2048,2048]{0,1:T(8,128)(2,1)} async-done(((bf16[256,2048]{0,1:T(8,128)(2,1)}), bf16[2048,2048]{0,1:T(8,128)(2,1)}) %all-gather.6.cloned.1.call-update) | async-done | bytes 8388624 | tf_op jit(solution)/shard_map/all_gather | solution.py:16
  289.0 16.5 %convolution_convert_fusion = bf16[512,2048]{1,0:T(8,128)(2,1)} fusion(bf16[2048,2048]{0,1:T(8,128)(2,1)} %all-gather.6.cloned.1.call-done, bf16[512,2048]{1,0:T(8,128)(2,1)} %all-gather.8.cloned.1.call-done, bf16[2048,2048]{1,0:T(8,128)(2,1)} %all-gather.4.cloned.1.call-done), kind=kOutput, calls=%fused_computation.1 | convolution fusion | flops 8594128896 | bytes 20971520 | tf_op jit(solution)/shard_map/dot_general | solution.py:25
  305.5 0.0 reduce-scatter.2.cloned.1.call-update
  305.6 29.5 %reduce-scatter.2.cloned.1.call-done = bf16[128,2048]{1,0:T(8,128)(2,1)} async-done(((bf16[512,2048]{1,0:T(8,128)(2,1)}), bf16[128,2048]{1,0:T(8,128)(2,1)}) %reduce-scatter.2.cloned.1.call-update) | async-done | bytes 524304 | tf_op jit(solution)/shard_map/reduce_scatter | solution.py:24
  335.0 8.4 %copy.10 = bf16[2048,2048]{1,0:T(8,128)(2,1)} copy(bf16[2048,2048]{1,0:T(8,128)(2,1)} %all-gather.4.cloned.1.call-done) | data formatting | bytes 16777216
  343.5 8.4 %copy.11 = bf16[2048,2048]{1,0:T(8,128)(2,1)} copy(bf16[2048,2048]{1,0:T(8,128)(2,1)} %bitcast.4) | data formatting | bytes 16777216
  (1 shorter events, 0.0 us)
Async XLA Ops:
  7.2 6.3 %copy-start = (f32[256,2048]{1,0:T(8,128)S(1)}, f32[256,2048]{1,0:T(8,128)}, u32[]{:S(2)}) copy-start(f32[256,2048]{1,0:T(8,128)} %param.7) | copy-start | bytes 6291460
  7.2 28.9 %all-gather.8.cloned.1.call-start = ((), (), s32[]{:S(2)}) async-start(), calls=%async_computation.3 | async-start | bytes 2621440 | tf_op jit(solution)/shard_map/all_gather | solution.py:13
  10.6 152.6 %all-gather.4.cloned.1.call-start = ((), (), s32[]{:S(2)}) async-start(), calls=%async_computation.1 | async-start | bytes 9437184 | tf_op jit(solution)/shard_map/all_gather | solution.py:15
  13.4 275.6 %all-gather.6.cloned.1.call-start = ((), (), s32[]{:S(2)}) async-start(), calls=%async_computation.2 | async-start | bytes 9437184 | tf_op jit(solution)/shard_map/all_gather | solution.py:16
  14.9 320.2 %reduce-scatter.2.cloned.1.call-start = ((), (), s32[]{:S(2)}) async-start(), calls=%async_computation.4 | async-start | bytes 2621440 | tf_op jit(solution)/shard_map/reduce_scatter | solution.py:24
Sparse Core Ops, SparseCore 0:
  10.7 25.2 all-gather.7
  38.8 124.4 all-gather.3
  165.9 123.1 all-gather.5
  305.7 29.3 reduce-scatter.1
where the time goes:
time: 359 us; the launch traced here: 358 us
  waiting for transfers between devices  304 us (85%)
  local copies, waits for them, and re-layouts  18.3 us (5%)
  matrix products  16.5 us (5%)
  between operations  13.8 us (4%)
  other arithmetic  6.11 us (2%)
    all_gather x1, waiting for transfers between devices, shards(): lax.all_gather(up_local, 'fs', axis=0, tiled=True)  127 us
    all_gather x1, waiting for transfers between devices, shards(): lax.all_gather(down_local, 'fs', axis=0, tiled=True)  126 us
    reduce_scatter x1, waiting for transfers between devices, shards(): lax.psum_scatter(jnp.dot(hidden, down_served, preferred_element_type=jnp....  29.5 us
    all_gather x1, waiting for transfers between devices, shards(): group_rows = lax.all_gather(normed, 'tp', axis=0, tiled=True)  21.1 us
    unnamed x5, local copies, waits for them, and re-layouts  18.3 us
    dot_general x1, matrix products, shards(): jnp.dot(hidden, down_served, preferred_element_type=jnp.float32)  16.5 us
  transfers between devices with their start and end apart: 4, of which 4 were waited for; matrix products, arithmetic and copies ran while one was open for 1% of the time, Pallas kernels for 0%

commit v1 on v0

--- a/solution.py
+++ b/solution.py
@@ -10,7 +10,14 @@
     values = prompt.astype(jnp.float32)
     scale = lax.rsqrt(jnp.mean(values * values, axis=-1, keepdims=True) + 1e-06)
     normed = (values * scale).astype(jnp.bfloat16)
-    group_rows = lax.all_gather(normed, "tp", axis=0, tiled=True)
+    peers = lax.axis_size("tp")
+    right = [(i, (i + 1) % peers) for i in range(peers)]
+    parts = [normed]
+    for hop in range(1, peers):
+        parts = [lax.ppermute(parts[0], "tp", right), *parts]
+    whole = jnp.concatenate(parts, axis=0)
+    offset = (lax.axis_index("tp") + 1) * parts[-1].shape[0]
+    group_rows = jnp.roll(whole, offset, axis=0)
     pieces = (
         lax.all_gather(up_local, "fs", axis=0, tiled=True),
         lax.all_gather(down_local, "fs", axis=0, tiled=True),

time: 359 us -> 333 us (0.928)
  waiting for transfers between devices: 304 us -> 273 us
  local copies, waits for them, and re-layouts: 18.3 us -> 23.2 us
    all_gather x1, waiting for transfers between devices: 127 us -> 92.5 us  [shards(): lax.all_gather(up_local, 'fs', axis=0, tiled=True)]
    ppermute x0 -> x3, waiting for transfers between devices: none -> 26 us  [shards(): parts = [lax.ppermute(parts[0], 'tp', right), *parts]]
    all_gather x1 -> x0, waiting for transfers between devices: 21.1 us -> none  [shards(): group_rows = lax.all_gather(normed, 'tp', axis=0, tiled=True)]
    unnamed x5 -> x13, local copies, waits for them, and re-layouts: 18.3 us -> 23.2 us
  transfers between devices with their start and end apart: 4 -> 6, of which waited for: 4 -> 6; matrix products, arithmetic and copies ran while one was open for 1% -> 3% of each run, Pallas kernels for 0% -> 0%
where the time goes in v1:
time: 333 us
  waiting for transfers between devices  273 us (82%)
  local copies, waits for them, and re-layouts  23.2 us (7%)
  matrix products  16.5 us (5%)
  between operations  13.8 us (4%)
  other arithmetic  5.14 us (2%)
    all_gather x1, waiting for transfers between devices, shards(): lax.all_gather(down_local, 'fs', axis=0, tiled=True)  125 us
    all_gather x1, waiting for transfers between devices, shards(): lax.all_gather(up_local, 'fs', axis=0, tiled=True)  92.5 us
    reduce_scatter x1, waiting for transfers between devices, shards(): lax.psum_scatter(jnp.dot(hidden, down_served, preferred_element_type=jnp....  29.5 us
    ppermute x3, waiting for transfers between devices, shards(): parts = [lax.ppermute(parts[0], 'tp', right), *parts]  26 us
    unnamed x13, local copies, waits for them, and re-layouts  23.2 us
    dot_general x1, matrix products, shards(): jnp.dot(hidden, down_served, preferred_element_type=jnp.float32)  16.5 us
  transfers between devices with their start and end apart: 6, of which 6 were waited for; matrix products, arithmetic and copies ran while one was open for 3% of the time, Pallas kernels for 0%

profile of v1, /device:TPU:0, one launch (start us, length us, event | category | flops | bytes accessed | tf_op | source)
XLA Modules:
  0.0 332.5 jit_solution(10200360888882709802)
XLA Ops:
  7.2 2.9 multiply_convert_fusion.1
  10.1 0.0 all-gather.5.cloned.1.call-start
  10.2 1.4 copy.7
  11.6 0.0 reduce-scatter.2.cloned.1.call-start
  11.7 0.2 fusion.1
  11.9 0.2 fusion.2
  12.0 0.5 collective-permute-start
  12.6 8.8 %collective-permute-done = bf16[128,2048]{1,0:T(8,128)(2,1)S(1)} collective-permute-done((bf16[128,2048]{1,0:T(8,128)(2,1)S(1)}, bf16[128,2048]{1,0:T(8,128)(2,1)S(1)}, u32[]{:S(2)}, u32[]{:S(2)}) %collective-permute-start) | collective-permute-done | bytes 524320 | tf_op jit(solution)/shard_map/ppermute | solution.py:17
  21.4 8.6 %collective-permute-done.1 = bf16[128,2048]{1,0:T(8,128)(2,1)S(1)} collective-permute-done((bf16[128,2048]{1,0:T(8,128)(2,1)S(1)}, bf16[128,2048]{1,0:T(8,128)(2,1)S(1)}, u32[]{:S(2)}, u32[]{:S(2)}) %collective-permute-start.1) | collective-permute-done | bytes 524320 | tf_op jit(solution)/shard_map/ppermute | solution.py:17
  30.0 8.6 %collective-permute-done.2 = bf16[128,2048]{1,0:T(8,128)(2,1)S(1)} collective-permute-done((bf16[128,2048]{1,0:T(8,128)(2,1)S(1)}, bf16[128,2048]{1,0:T(8,128)(2,1)S(1)}, u32[]{:S(2)}, u32[]{:S(2)}) %collective-permute-start.2) | collective-permute-done | bytes 524320 | tf_op jit(solution)/shard_map/ppermute | solution.py:17
  38.6 0.8 constant_dynamic-update-slice_fusion.7
  39.4 0.8 constant_dynamic-update-slice_fusion.6
  40.2 0.8 constant_dynamic-update-slice_fusion.5
  41.1 0.9 constant_dynamic-update-slice_fusion.4
  42.0 0.8 constant_dynamic-update-slice_fusion.3
  42.8 0.8 constant_dynamic-update-slice_fusion.2
  43.7 0.8 constant_dynamic-update-slice_fusion.1
  44.5 0.9 constant_dynamic-update-slice_fusion
  45.4 92.5 %all-gather.3.cloned.1.call-done = bf16[2048,2048]{1,0:T(8,128)(2,1)} async-done(((bf16[256,2048]{1,0:T(8,128)(2,1)}), bf16[2048,2048]{1,0:T(8,128)(2,1)}) %all-gather.3.cloned.1.call-update) | async-done | bytes 8388624 | tf_op jit(solution)/shard_map/all_gather | solution.py:22
  137.9 125.2 %all-gather.5.cloned.1.call-done = bf16[2048,2048]{0,1:T(8,128)(2,1)} async-done(((bf16[256,2048]{0,1:T(8,128)(2,1)}), bf16[2048,2048]{0,1:T(8,128)(2,1)}) %all-gather.5.cloned.1.call-update) | async-done | bytes 8388624 | tf_op jit(solution)/shard_map/all_gather | solution.py:23
  263.1 16.5 %convolution_convert_fusion = bf16[512,2048]{1,0:T(8,128)(2,1)} fusion(bf16[2048,2048]{0,1:T(8,128)(2,1)} %all-gather.5.cloned.1.call-done, bf16[2048,2048]{1,0:T(8,128)(2,1)} %all-gather.3.cloned.1.call-done, bf16[1024,2048]{1,0:T(8,128)(2,1)} %constant_dynamic-update-slice_fusion, s32[]{:T(128)S(6)} %select_n.14), kind=kOutput, calls=%fused_computation.1 | convolution fusion | flops 8594128896 | bytes 20971524 | tf_op jit(solution)/shard_map/dot_general | solution.py:32
  279.6 29.5 %reduce-scatter.2.cloned.1.call-done = bf16[128,2048]{1,0:T(8,128)(2,1)} async-done(((bf16[512,2048]{1,0:T(8,128)(2,1)}), bf16[128,2048]{1,0:T(8,128)(2,1)}) %reduce-scatter.2.cloned.1.call-update) | async-done | bytes 524304 | tf_op jit(solution)/shard_map/reduce_scatter | solution.py:31
  309.1 8.4 %copy.17 = bf16[2048,2048]{1,0:T(8,128)(2,1)} copy(bf16[2048,2048]{1,0:T(8,128)(2,1)} %all-gather.3.cloned.1.call-done) | data formatting | bytes 16777216
  317.6 8.4 %copy.18 = bf16[2048,2048]{1,0:T(8,128)(2,1)} copy(bf16[2048,2048]{1,0:T(8,128)(2,1)} %bitcast.8) | data formatting | bytes 16777216
  (11 shorter events, 0.1 us)
Async XLA Ops:
  7.2 3.0 copy-start.1
  7.2 4.5 %copy-start = (bf16[128,2048]{1,0:T(8,128)(2,1)S(1)}, bf16[128,2048]{1,0:T(8,128)(2,1)}, u32[]{:S(2)}) copy-start(bf16[128,2048]{1,0:T(8,128)(2,1)} %param.4) | copy-start | bytes 1572868
  7.2 130.7 %all-gather.3.cloned.1.call-start = ((), (), s32[]{:S(2)}) async-start(), calls=%async_computation.1 | async-start | bytes 9437184 | tf_op jit(solution)/shard_map/all_gather | solution.py:22
  10.1 253.0 %all-gather.5.cloned.1.call-start = ((), (), s32[]{:S(2)}) async-start(), calls=%async_computation.2 | async-start | bytes 9437184 | tf_op jit(solution)/shard_map/all_gather | solution.py:23
  11.6 297.5 %reduce-scatter.2.cloned.1.call-start = ((), (), s32[]{:S(2)}) async-start(), calls=%async_computation.3 | async-start | bytes 2621440 | tf_op jit(solution)/shard_map/reduce_scatter | solution.py:31
  12.0 9.3 %collective-permute-start = (bf16[128,2048]{1,0:T(8,128)(2,1)S(1)}, bf16[128,2048]{1,0:T(8,128)(2,1)S(1)}, u32[]{:S(2)}, u32[]{:S(2)}) collective-permute-start(bf16[128,2048]{1,0:T(8,128)(2,1)S(1)} %fusion.2), channel_id=1, source_target_pairs={{0,1},{1,2},{2,3},{3,0},{4,5},{5,6},{6,7},{7,4},{8,9},{9,10},{10,1... | collective-permute-start | bytes 1572872 | tf_op jit(solution)/shard_map/ppermute | solution.py:17
  21.4 8.6 %collective-permute-start.1 = (bf16[128,2048]{1,0:T(8,128)(2,1)S(1)}, bf16[128,2048]{1,0:T(8,128)(2,1)S(1)}, u32[]{:S(2)}, u32[]{:S(2)}) collective-permute-start(bf16[128,2048]{1,0:T(8,128)(2,1)S(1)} %collective-permute-done), channel_id=1, source_target_pairs={{0,1},{1,2},{2,3},{3,0},{4,5},{5,6},{6,7},{7,4},{8,9},{9,10},{10,1... | collective-permute-start | bytes 1572872 | tf_op jit(solution)/shard_map/ppermute | solution.py:17
  30.0 8.6 %collective-permute-start.2 = (bf16[128,2048]{1,0:T(8,128)(2,1)S(1)}, bf16[128,2048]{1,0:T(8,128)(2,1)S(1)}, u32[]{:S(2)}, u32[]{:S(2)}) collective-permute-start(bf16[128,2048]{1,0:T(8,128)(2,1)S(1)} %collective-permute-done.1), channel_id=1, source_target_pairs={{0,1},{1,2},{2,3},{3,0},{4,5},{5,6},{6,7},{7,4},{8,9},{9,10},{10,1... | collective-permute-start | bytes 1572872 | tf_op jit(solution)/shard_map/ppermute | solution.py:17
Sparse Core Ops, SparseCore 0:
  10.7 127.1 all-gather.2
  140.0 123.1 all-gather.4
  279.8 29.3 reduce-scatter.1
